TPU v7x, 32 devices: a whole 2x2x4 slice. The times are simulated.
32 devices in a mesh: kv: 8 (over z, y), tp: 4 (over x, core).
Axes of the slice: x: 2, y: 2, z: 4, core: 2. Of those that a mesh axis runs over, the one named last changes fastest.
Arguments:
- tokens: bfloat16 [16, 4096], P(None, ('kv', 'tp')), may hold values from -6 to 6
- gain_attn: bfloat16 [4096], replicated, may hold values from 0.099609375 to 1.8984375
- w_query: bfloat16 [4096, 2048], P('kv', 'tp'), may hold values from -0.09375 to 0.09375
- w_key: bfloat16 [4096, 2048], P('kv', 'tp'), may hold values from -0.09375 to 0.09375
- w_value: bfloat16 [4096, 2048], P('kv', 'tp'), may hold values from -0.09375 to 0.09375
- w_forget: bfloat16 [4096, 32], replicated, may hold values from -0.09375 to 0.09375
- forget_bias: float32 [32], replicated, may hold values from -2 to 2
- keys_cache: bfloat16 [16, 4096, 2048], P(None, 'kv', 'tp'), may hold values from -900 to 900
- values_cache: bfloat16 [16, 4096, 2048], P(None, 'kv', 'tp'), may hold values from -6 to 6
- gates_cache: float32 [16, 32, 4096], P(None, 'tp', 'kv'), as said below
- lengths: int32 [16], replicated, may hold values from 1 to 4096, 32768 in all
- w_out: bfloat16 [2048, 4096], P('tp', 'kv'), may hold values from -0.1875 to 0.1875
- gain_mixer: bfloat16 [4096], replicated, may hold values from 0.099609375 to 1.8984375
- w_up: bfloat16 [4096, 16384], P('kv', 'tp'), may hold values from -0.09375 to 0.09375
- w_down: bfloat16 [16384, 4096], P('tp', 'kv'), may hold values from -0.0625 to 0.0625
Outputs:
- output: bfloat16 [16, 4096], P(None, ('kv', 'tp'))
Inputs may be any that keep to these rules, and one draw needn't show every extreme that they name: One sequence has all 4096 positions live; the lengths add up to half of 16 times 4096. `gates_cache`: along positions each entry is the running sum of per-position log forget gates up to and including that position, so the values never rise.
All inputs are finite; a program needn't handle non-finite values.
Results may differ from a plain program's by a relative error of at most 0.017.
Values may be sent and summed in bfloat16 or wider, within the bound.
A program may use at most 128 MiB of HBM per device.

v0:
```python
import functools

import jax
import jax.numpy as jnp
from jax import lax
from jax.experimental import pallas as pl
from jax.experimental.pallas import tpu as pltpu
from jax.sharding import PartitionSpec as P

norm_eps = 1e-06


def combined_all(value, axis, join):
    pieces = jax.tree.map(lambda part: lax.all_gather(part, axis), value)
    head = jax.tree.map(lambda part: part[0], pieces)
    tail = jax.tree.map(lambda part: part[1:], pieces)
    total, _ = lax.scan(lambda total, section: (join(total, section), None), head, tail)
    return total


def combine_parts(earlier, later):
    top = jnp.maximum(earlier[0], later[0])
    early_factor = jnp.exp(earlier[0] - top)
    late_factor = jnp.exp(later[0] - top)
    totals = earlier[1] * early_factor + later[1] * late_factor
    summed = earlier[2] * early_factor[..., None] + later[2] * late_factor[..., None]
    return (top, totals, summed, earlier[3] + later[3])


def channel_mix(residual, gain_mixer, w_up, w_down, kv_index):
    width = gain_mixer.shape[0]
    block_start = kv_index * w_up.shape[0]
    piece = lax.all_gather(residual, "tp", axis=1, tiled=True)
    piece_f = piece.astype(jnp.float32)
    gain_part = lax.dynamic_slice_in_dim(gain_mixer, block_start, piece.shape[1], 0).astype(
        jnp.float32
    )
    scaled = (piece_f * gain_part).astype(jnp.bfloat16)
    upward = jnp.dot(scaled, w_up, preferred_element_type=jnp.float32)
    upward, squares = (upward, jnp.sum(piece_f * piece_f, axis=-1))
    up_total, square_total = lax.psum((upward, squares), "kv")
    mixer_scale = lax.rsqrt(square_total / width + norm_eps)
    active = jax.nn.relu(mixer_scale[:, None] * up_total)
    hidden = (active * active).astype(jnp.bfloat16)
    down = jnp.dot(hidden, w_down, preferred_element_type=jnp.float32)
    return lax.psum_scatter(down, "tp", scatter_dimension=1, tiled=True)


def shards(
    tokens,
    gain_attn,
    w_query,
    w_key,
    w_value,
    w_forget,
    forget_bias,
    keys_cache,
    values_cache,
    gates_cache,
    lengths,
    w_out,
    gain_mixer,
    w_up,
    w_down,
):
    kv_index = lax.axis_index("kv")
    tp_index = lax.axis_index("tp")
    row_block = w_query.shape[0]
    heads_here = gates_cache.shape[1]
    width = gain_attn.shape[0]
    row_start = kv_index * row_block
    head_start = tp_index * heads_here
    block_raw = lax.all_gather(tokens, "tp", axis=1, tiled=True)
    block_f = block_raw.astype(jnp.float32)
    gain_block = lax.dynamic_slice_in_dim(gain_attn, row_start, row_block, 0).astype(jnp.float32)
    block = (block_f * gain_block).astype(jnp.bfloat16)
    forget_block = lax.dynamic_slice(w_forget, (row_start, head_start), (row_block, heads_here))
    part_query = jnp.dot(block, w_query, preferred_element_type=jnp.float32)
    part_key = jnp.dot(block, w_key, preferred_element_type=jnp.float32)
    part_value = jnp.dot(block, w_value, preferred_element_type=jnp.float32)
    part_gate = jnp.dot(block, forget_block, preferred_element_type=jnp.float32)
    part_squares = jnp.sum(block_f * block_f, axis=-1)
    sum_query, sum_key, sum_value, sum_gate, squares = lax.psum(
        (part_query, part_key, part_value, part_gate, part_squares), "kv"
    )
    attn_scale = lax.rsqrt(squares / width + norm_eps)[:, None]
    gate_logit = attn_scale * sum_gate
    query = (attn_scale * sum_query).astype(jnp.bfloat16)
    new_key = (attn_scale * sum_key).astype(jnp.bfloat16)
    new_value = (attn_scale * sum_value).astype(jnp.bfloat16)
    bias_here = lax.dynamic_slice_in_dim(forget_bias, head_start, heads_here, 0)
    forget_log = jax.nn.log_sigmoid(gate_logit + bias_here)
    seqs = tokens.shape[0]
    positions_here = keys_cache.shape[1]
    query_heads = query.reshape(seqs, heads_here, -1)
    head_size = query_heads.shape[-1]
    keys_heads = keys_cache.reshape(seqs, positions_here, heads_here, head_size)
    values_heads = values_cache.reshape(seqs, positions_here, heads_here, head_size)
    scores = jnp.einsum(
        "bhd,bphd->bhp", query_heads, keys_heads, preferred_element_type=jnp.float32
    )
    logits = scores * head_size ** (-0.5) - gates_cache
    positions = kv_index * positions_here + jnp.arange(positions_here, dtype=jnp.int32)
    valid = (positions[None, :] < lengths[:, None])[:, None, :]
    local_top = jnp.max(jnp.where(valid, logits, -1e30), axis=-1)
    weights = jnp.where(valid, jnp.exp(logits - local_top[..., None]), 0.0)
    local_total = jnp.sum(weights, axis=-1)
    local_sum = jnp.einsum(
        "bhp,bphd->bhd",
        weights.astype(jnp.bfloat16),
        values_heads,
        preferred_element_type=jnp.float32,
    )
    at_last = (positions[None, :] == lengths[:, None] - 1)[:, None, :]
    last_local = jnp.sum(jnp.where(at_last, gates_cache, 0.0), axis=-1)
    top, totals, summed, last_gate = combined_all(
        (local_top, local_total, local_sum, last_local), "kv", combine_parts
    )
    top = top + last_gate + forget_log
    own = jnp.sum(
        query_heads.astype(jnp.float32) * new_key.reshape(seqs, heads_here, -1).astype(jnp.float32),
        axis=-1,
    ) * head_size ** (-0.5)
    overall = jnp.maximum(top, own)
    cache_factor = jnp.exp(top - overall)
    own_weight = jnp.exp(own - overall)
    denominator = totals * cache_factor + own_weight
    numerator = summed * cache_factor[..., None] + own_weight[..., None] * new_value.reshape(
        seqs, heads_here, -1
    ).astype(jnp.float32)
    mixed = (numerator / denominator[..., None]).astype(jnp.bfloat16).reshape(seqs, -1)
    partial_value = jnp.dot(mixed, w_out, preferred_element_type=jnp.float32).astype(jnp.bfloat16)
    attended = lax.psum_scatter(partial_value, "tp", scatter_dimension=1, tiled=True).astype(
        jnp.float32
    )
    residual = (tokens.astype(jnp.float32) + attended).astype(jnp.bfloat16)
    mixer = channel_mix(residual, gain_mixer, w_up, w_down, kv_index)
    return (residual.astype(jnp.float32) + mixer).astype(jnp.bfloat16)


f32, bf16 = jnp.float32, jnp.bfloat16
LANES = 128


def to_row(column):
    shape = (column.shape[0], LANES)
    same = lax.broadcasted_iota(jnp.int32, shape, 0) == lax.broadcasted_iota(jnp.int32, shape, 1)
    return jnp.sum(jnp.where(same, column, 0.0), axis=0, keepdims=True)


def to_column(row, count):
    shape = (count, LANES)
    same = lax.broadcasted_iota(jnp.int32, shape, 0) == lax.broadcasted_iota(jnp.int32, shape, 1)
    return jnp.sum(jnp.where(same, row, 0.0), axis=-1, keepdims=True)


def fused(
    n_kv,
    n_tp,
    tokens,
    gain_attn,
    forget_bias,
    lengths,
    gain_mixer,
    w_query,
    w_key,
    w_value,
    w_forget,
    keys_cache,
    values_cache,
    gates_cache,
    w_out,
    w_up,
    w_down,
    out,
    wq,
    wk,
    wv,
    wf,
    keys,
    values,
    gates,
    wo,
    wu,
    wd,
    tok_all,
    q_send,
    q_all,
    p_send,
    p_all,
    a_send,
    a_all,
    m_send,
    m_all,
    o_send,
    o_all,
    u_send,
    u_all,
    h_send,
    h_all,
    f_send,
    f_all,
    query,
    mix,
    res,
    s_send,
    s_all,
    load_sem,
    kv_out,
    kv_in,
    tp_out,
    tp_in,
):
    kv, tp = lax.axis_index("kv"), lax.axis_index("tp")
    seqs, piece = tokens.shape
    rows, cols = wq.shape
    positions = keys.shape[1]
    heads = gates.shape[1]
    all_heads = wf.shape[0]
    size = cols // heads
    mine = seqs // n_kv
    width = gain_attn.shape[0]
    unit = wu.shape[1] // n_kv

    row_at = pl.multiple_of(kv * rows, rows)
    sources = [
        (w_query, wq),
        (w_key, wk),
        (w_value, wv),
        (w_forget.at[:, pl.ds(row_at, rows)], wf),
        (keys_cache, keys),
        (gates_cache, gates),
        (values_cache, values),
        (w_out, wo),
        (w_up, wu),
        (w_down, wd),
    ]
    loads = [pltpu.make_async_copy(a, b, load_sem.at[i]) for i, (a, b) in enumerate(sources)]
    for load in loads:
        load.start()
    ld_q, ld_k, ld_v, ld_f, ld_keys, ld_gates, ld_values, ld_o, ld_u, ld_d = loads

    barrier = pltpu.get_barrier_semaphore()
    for j in range(1, n_kv):
        pl.semaphore_signal(
            barrier,
            inc=1,
            device_id=(lax.rem(kv + j, n_kv), tp),
            device_id_type=pl.DeviceIdType.MESH,
        )
    for j in range(1, n_tp):
        pl.semaphore_signal(
            barrier,
            inc=1,
            device_id=(kv, lax.rem(tp + j, n_tp)),
            device_id_type=pl.DeviceIdType.MESH,
        )
    pl.semaphore_wait(barrier, n_kv + n_tp - 2)

    turn = 2 * (kv // (n_kv // 2)) - 1

    def kv_peer(j):
        return lax.rem(kv + turn * j + n_kv, n_kv)

    def over_kv(phase, j, source, landing):
        peer = kv_peer(j)
        return pltpu.make_async_remote_copy(
            src_ref=source(peer),
            dst_ref=landing.at[kv],
            send_sem=kv_out.at[phase, j],
            recv_sem=kv_in.at[phase, kv],
            device_id=(peer, tp),
            device_id_type=pl.DeviceIdType.MESH,
        )

    def from_kv(phase, j, source, landing):
        peer = lax.rem(kv - turn * j + n_kv, n_kv)
        pltpu.make_async_remote_copy(
            src_ref=source(peer),
            dst_ref=landing.at[peer],
            send_sem=kv_out.at[phase, j],
            recv_sem=kv_in.at[phase, peer],
            device_id=(peer, tp),
            device_id_type=pl.DeviceIdType.MESH,
        ).wait_recv()
        return peer

    def over_tp(phase, j, source, landing):
        peer = lax.rem(tp + j, n_tp)
        return pltpu.make_async_remote_copy(
            src_ref=source(peer),
            dst_ref=landing.at[tp],
            send_sem=tp_out.at[phase, j],
            recv_sem=tp_in.at[phase, tp],
            device_id=(kv, peer),
            device_id_type=pl.DeviceIdType.MESH,
        )

    def from_tp(phase, j, source, landing):
        peer = lax.rem(tp + n_tp - j, n_tp)
        pltpu.make_async_remote_copy(
            src_ref=source(peer),
            dst_ref=landing.at[peer],
            send_sem=tp_out.at[phase, j],
            recv_sem=tp_in.at[phase, peer],
            device_id=(kv, peer),
            device_id_type=pl.DeviceIdType.MESH,
        ).wait_recv()
        return peer

    pending = []

    def send_kv(phase, j, source, landing):
        copy = over_kv(phase, j, source, landing)
        copy.start()
        pending.append(copy)

    def send_tp(phase, j, source, landing):
        copy = over_tp(phase, j, source, landing)
        copy.start()
        pending.append(copy)

    def share_squares(which, block):
        column = jnp.sum(block * block, axis=-1, keepdims=True)
        s_send[which] = to_row(column)
        for j in range(1, n_kv):
            send_kv(6 + which, j, lambda peer: s_send.at[which], s_all.at[which])
        s_all[which, kv] = s_send[which]

    def joined_squares(which):
        for j in range(1, n_kv):
            from_kv(6 + which, j, lambda peer: s_send.at[which], s_all.at[which])
        total = s_all[which, 0]
        for o in range(1, n_kv):
            total = total + s_all[which, o]
        return to_column(total, seqs)

    for j in range(1, n_tp):
        send_tp(0, j, lambda peer: tokens, tok_all)
    tok_all[tp] = tokens[...]
    gain_a = gain_attn[pl.ds(row_at, rows)].astype(f32).reshape(1, rows)
    gain_m = gain_mixer[pl.ds(row_at, rows)].astype(f32).reshape(1, rows)
    for j in range(1, n_tp):
        from_tp(0, j, lambda peer: tokens, tok_all)
    tok = jnp.concatenate([tok_all[t] for t in range(n_tp)], axis=1).astype(f32)
    scaled = (tok * gain_a).astype(bf16)

    share_squares(0, tok)

    ld_q.wait()
    q_send[...] = jnp.dot(scaled, wq[...], preferred_element_type=f32).astype(bf16)
    for j in range(1, n_kv):
        send_kv(0, j, lambda peer: q_send, q_all)
    q_all[kv] = q_send[...]

    ld_k.wait()
    ld_v.wait()
    ld_f.wait()
    part_key = jnp.dot(scaled, wk[...], preferred_element_type=f32)
    part_value = jnp.dot(scaled, wv[...], preferred_element_type=f32)
    part_gate = lax.dot_general(
        scaled, wf[...], (((1,), (1,)), ((), ())), preferred_element_type=f32
    )
    for o in range(n_kv):
        at = slice(o * mine, (o + 1) * mine)
        p_send[o, :, :cols] = part_key[at]
        p_send[o, :, cols : 2 * cols] = part_value[at]
        p_send[o, :, 2 * cols : 2 * cols + all_heads] = part_gate[at]
        p_send[o, :, 2 * cols + all_heads :] = jnp.zeros((mine, LANES - all_heads), f32)
    for j in range(1, n_kv):
        send_kv(1, j, lambda peer: p_send.at[peer], p_all)
    p_all[kv] = p_send[kv]

    for j in range(1, n_kv):
        from_kv(0, j, lambda peer: q_send, q_all)
    q_total = q_all[0].astype(f32)
    for o in range(1, n_kv):
        q_total = q_total + q_all[o].astype(f32)
    attn_scale = lax.rsqrt(joined_squares(0) / width + norm_eps)
    query[:, :cols] = (attn_scale * q_total).astype(bf16).astype(f32)
    query[:, cols:] = jnp.broadcast_to(attn_scale, (seqs, LANES))

    ld_keys.wait()
    ld_gates.wait()
    ld_values.wait()
    head_row = lax.broadcasted_iota(jnp.int32, (heads, cols), 0)
    own_block = head_row == lax.broadcasted_iota(jnp.int32, (heads, cols), 1) // size
    place = kv * positions + lax.broadcasted_iota(jnp.int32, (heads, positions), 1)
    stat_row = lax.broadcasted_iota(jnp.int32, (heads, LANES), 0)
    stat_lane = lax.broadcasted_iota(jnp.int32, (heads, LANES), 1)

    def attend(owner):
        for r in range(mine):
            b = owner * mine + r
            spread = jnp.where(own_block, query[pl.ds(b, 1), :cols], 0.0).astype(bf16)
            scores = lax.dot_general(
                spread, keys[b], (((1,), (1,)), ((), ())), preferred_element_type=f32
            )
            gate = gates[b]
            length = lengths[b]
            valid = place < length
            logits = scores * size ** (-0.5) - gate
            top = jnp.max(jnp.where(valid, logits, -1e30), axis=-1, keepdims=True)
            weights = jnp.where(valid, jnp.exp(logits - top), 0.0)
            total = jnp.sum(weights, axis=-1, keepdims=True)
            last = jnp.sum(jnp.where(place == length - 1, gate, 0.0), axis=-1, keepdims=True)
            summed = jnp.dot(weights.astype(bf16), values[b], preferred_element_type=f32)
            a_send[owner, r : r + 1, :cols] = jnp.sum(
                jnp.where(own_block, summed, 0.0), axis=0, keepdims=True
            )
            stats = jnp.where(
                stat_lane == stat_row,
                top,
                jnp.where(
                    stat_lane == stat_row + heads,
                    total,
                    jnp.where(stat_lane == stat_row + 2 * heads, last, 0.0),
                ),
            )
            a_send[owner, r : r + 1, cols:] = jnp.sum(stats, axis=0, keepdims=True)

    def attend_for(j, carry):
        attend(kv_peer(j))
        over_kv(2, j, lambda peer: a_send.at[peer], a_all).start()
        return carry

    lax.fori_loop(1, n_kv, attend_for, 0)
    attend(kv)
    a_all[kv] = a_send[kv]

    for j in range(1, n_kv):
        from_kv(1, j, lambda peer: p_send.at[peer], p_all)
    p_total = p_all[0]
    for o in range(1, n_kv):
        p_total = p_total + p_all[o]
    own_rows = [query[pl.ds(kv * mine + r, 1), :] for r in range(mine)]
    own_query = jnp.concatenate(own_rows, axis=0)
    own_scale = own_query[:, cols : cols + 1]
    own_query = own_query[:, :cols]
    new_key = (own_scale * p_total[:, :cols]).astype(bf16).astype(f32)
    new_value = (own_scale * p_total[:, cols : 2 * cols]).astype(bf16).astype(f32)
    gate_logit = own_scale * p_total[:, 2 * cols : 2 * cols + all_heads] + forget_bias[...]
    forget_log = jnp.minimum(gate_logit, 0.0) - jnp.log1p(jnp.exp(-jnp.abs(gate_logit)))
    col_head = lax.broadcasted_iota(jnp.int32, (mine, cols), 1) // size
    forget_wide = jnp.zeros((mine, cols), f32)
    for h in range(all_heads):
        forget_wide = jnp.where(col_head + tp * heads == h, forget_log[:, h : h + 1], forget_wide)
    product = own_query * new_key
    own = jnp.zeros((mine, cols), f32)
    for h in range(heads):
        inside = col_head == h
        own = jnp.where(
            inside, jnp.sum(jnp.where(inside, product, 0.0), axis=-1, keepdims=True), own
        )
    own = own * size ** (-0.5)

    for j in range(1, n_kv):
        from_kv(2, j, lambda peer: a_send.at[peer], a_all)

    def wide(part, first):
        result = jnp.zeros((mine, cols), f32)
        for h in range(heads):
            result = jnp.where(col_head == h, part[:, first + h : first + h + 1], result)
        return result

    tops = [wide(a_all[o, :, cols:], 0) for o in range(n_kv)]
    top = functools.reduce(jnp.maximum, tops)
    totals = jnp.zeros((mine, cols), f32)
    summed = jnp.zeros((mine, cols), f32)
    stat_sum = a_all[0, :, cols:]
    for o in range(1, n_kv):
        stat_sum = stat_sum + a_all[o, :, cols:]
    for o in range(n_kv):
        factor = jnp.exp(tops[o] - top)
        totals = totals + factor * wide(a_all[o, :, cols:], heads)
        summed = summed + factor * a_all[o, :, :cols]
    top = top + wide(stat_sum, 2 * heads) + forget_wide
    overall = jnp.maximum(top, own)
    cache_factor = jnp.exp(top - overall)
    own_weight = jnp.exp(own - overall)
    denominator = totals * cache_factor + own_weight
    numerator = summed * cache_factor + own_weight * new_value
    m_send[...] = (numerator / denominator).astype(bf16).astype(f32)
    for j in range(1, n_kv):
        send_kv(3, j, lambda peer: m_send, m_all)
    m_all[kv] = m_send[...]
    ld_o.wait()
    for j in range(1, n_kv):
        from_kv(3, j, lambda peer: m_send, m_all)
    for o in range(n_kv):
        mix[o * mine : (o + 1) * mine, :] = m_all[o]

    o_send[...] = jnp.dot(mix[...].astype(bf16), wo[...], preferred_element_type=f32).astype(bf16)
    for j in range(1, n_tp):
        send_tp(1, j, lambda peer: o_send, o_all)
    o_all[tp] = o_send[...]
    ld_u.wait()
    for j in range(1, n_tp):
        from_tp(1, j, lambda peer: o_send, o_all)
    attended = o_all[0].astype(f32)
    for t in range(1, n_tp):
        attended = attended + o_all[t].astype(f32)
    residual = (tok + attended).astype(bf16).astype(f32)
    for t in range(n_tp):
        res[t] = residual[:, t * piece : (t + 1) * piece]

    scaled_mid = (residual * gain_m).astype(bf16)
    share_squares(1, residual)

    def up_piece(owner):
        at = pl.multiple_of(owner * unit, unit)
        u_send[owner] = jnp.dot(
            scaled_mid, wu[:, pl.ds(at, unit)], preferred_element_type=f32
        ).astype(bf16)

    for j in range(1, n_kv):
        up_piece(kv_peer(j))
        send_kv(4, j, lambda peer: u_send.at[peer], u_all)
    up_piece(kv)
    u_all[kv] = u_send[kv]
    for j in range(1, n_kv):
        from_kv(4, j, lambda peer: u_send.at[peer], u_all)
    up_total = u_all[0].astype(f32)
    for o in range(1, n_kv):
        up_total = up_total + u_all[o].astype(f32)
    mixer_scale = lax.rsqrt(joined_squares(1) / width + norm_eps)
    active = jnp.maximum(mixer_scale * up_total, 0.0)
    h_send[...] = (active * active).astype(bf16)
    for j in range(1, n_kv):
        send_kv(5, j, lambda peer: h_send, h_all)

    ld_d.wait()

    def down_piece(block, owner):
        at = pl.multiple_of(owner * unit, unit)
        return jnp.dot(block, wd[pl.ds(at, unit), :], preferred_element_type=f32)

    down = down_piece(h_send[...], kv)
    for j in range(1, n_kv):
        peer = from_kv(5, j, lambda peer: h_send, h_all)
        down = down + down_piece(h_all[peer], peer)
    for t in range(n_tp):
        f_send[t] = down[:, t * piece : (t + 1) * piece]
    for j in range(1, n_tp):
        send_tp(2, j, lambda peer: f_send.at[peer], f_all)
    f_all[tp] = f_send[tp]
    for j in range(1, n_tp):
        from_tp(2, j, lambda peer: f_send.at[peer], f_all)
    mixer = f_all[0]
    for t in range(1, n_tp):
        mixer = mixer + f_all[t]
    out[...] = (res[tp] + mixer).astype(bf16)

    for copy in pending:
        copy.wait_send()
    for j in range(1, n_kv):
        over_kv(2, j, lambda peer: a_send.at[peer], a_all).wait_send()


def layer(n_kv, n_tp, *arrays):
    (
        tokens,
        gain_attn,
        w_query,
        w_key,
        w_value,
        w_forget,
        forget_bias,
        keys_cache,
        values_cache,
        gates_cache,
        lengths,
        w_out,
        gain_mixer,
        w_up,
        w_down,
    ) = arrays
    seqs, piece = tokens.shape
    rows, cols = w_query.shape
    heads = gates_cache.shape[1]
    all_heads = w_forget.shape[1]
    unit = w_up.shape[1] // n_kv
    fits = (
        piece % LANES == 0
        and cols % LANES == 0
        and unit % LANES == 0
        and seqs % n_kv == 0
        and 3 * heads <= LANES
        and all_heads < LANES
        and w_out.shape == (cols, rows)
        and seqs <= LANES
        and n_kv % 2 == 0
        and n_tp > 1
    )
    if not fits:
        return shards(*arrays)
    mine = seqs // n_kv
    vmem = pl.BlockSpec(memory_space=pltpu.VMEM)
    smem = pl.BlockSpec(memory_space=pltpu.SMEM)
    anywhere = pl.BlockSpec(memory_space=pl.ANY)

    def like(x):
        return pltpu.VMEM(x.shape, x.dtype)

    return pl.pallas_call(
        functools.partial(fused, n_kv, n_tp),
        out_shape=jax.ShapeDtypeStruct((seqs, piece), bf16),
        in_specs=[vmem, vmem, vmem, smem, vmem] + [anywhere] * 10,
        out_specs=vmem,
        scratch_shapes=[
            like(w_query),
            like(w_key),
            like(w_value),
            pltpu.VMEM((all_heads, rows), bf16),
            like(keys_cache),
            like(values_cache),
            like(gates_cache),
            like(w_out),
            like(w_up),
            like(w_down),
            pltpu.VMEM((n_tp, seqs, piece), bf16),
            pltpu.VMEM((seqs, cols), bf16),
            pltpu.VMEM((n_kv, seqs, cols), bf16),
            pltpu.VMEM((n_kv, mine, 2 * cols + LANES), f32),
            pltpu.VMEM((n_kv, mine, 2 * cols + LANES), f32),
            pltpu.VMEM((n_kv, mine, cols + LANES), f32),
            pltpu.VMEM((n_kv, mine, cols + LANES), f32),
            pltpu.VMEM((mine, cols), f32),
            pltpu.VMEM((n_kv, mine, cols), f32),
            pltpu.VMEM((seqs, rows), bf16),
            pltpu.VMEM((n_tp, seqs, rows), bf16),
            pltpu.VMEM((n_kv, seqs, unit), bf16),
            pltpu.VMEM((n_kv, seqs, unit), bf16),
            pltpu.VMEM((seqs, unit), bf16),
            pltpu.VMEM((n_kv, seqs, unit), bf16),
            pltpu.VMEM((n_tp, seqs, piece), f32),
            pltpu.VMEM((n_tp, seqs, piece), f32),
            pltpu.VMEM((seqs, cols + LANES), f32),
            pltpu.VMEM((seqs, cols), f32),
            pltpu.VMEM((n_tp, seqs, piece), f32),
            pltpu.VMEM((2, 1, LANES), f32),
            pltpu.VMEM((2, n_kv, 1, LANES), f32),
            pltpu.SemaphoreType.DMA((10,)),
            pltpu.SemaphoreType.DMA((8, n_kv)),
            pltpu.SemaphoreType.DMA((8, n_kv)),
            pltpu.SemaphoreType.DMA((3, n_tp)),
            pltpu.SemaphoreType.DMA((3, n_tp)),
        ],
        compiler_params=pltpu.CompilerParams(
            collective_id=0, has_side_effects=True, vmem_limit_bytes=60 * 1024 * 1024
        ),
    )(
        tokens,
        gain_attn,
        forget_bias.reshape(1, -1),
        lengths,
        gain_mixer,
        w_query,
        w_key,
        w_value,
        w_forget.T,
        keys_cache,
        values_cache,
        gates_cache,
        w_out,
        w_up,
        w_down,
    )


def solution(mesh):
    return jax.shard_map(
        functools.partial(layer, mesh.shape["kv"], mesh.shape["tp"]),
        mesh=mesh,
        in_specs=(
            P(None, ("kv", "tp")),
            P(),
            P("kv", "tp"),
            P("kv", "tp"),
            P("kv", "tp"),
            P(),
            P(),
            P(None, "kv", "tp"),
            P(None, "kv", "tp"),
            P(None, "tp", "kv"),
            P(),
            P("tp", "kv"),
            P(),
            P("kv", "tp"),
            P("tp", "kv"),
        ),
        out_specs=P(None, ("kv", "tp")),
        check_vma=False,
    )
```

profile of v0, /device:TPU:0, one launch (start us, length us, event | category | flops | bytes accessed | tf_op | source)
XLA Modules:
  0.0 48.1 jit_solution(16426859902299900190)
XLA Ops:
  0.0 46.8 %shard_map.145 = bf16[16,128]{1,0:T(8,128)(2,1)} custom-call(bf16[16,128]{1,0:T(8,128)(2,1)} %tokens.1, bf16[4096]{0:T(1024)(128)(2,1)} %gain_attn.1, f32[1,32]{1,0:T(1,128)} %bitcast.3, s32[16]{0:T(128)} %lengths.1, bf16[4096]{0:T(1024)(128)(2,1)} %gain_mixer.1, bf16[512,512]{1,0:T(8,128)(2,1)} %w_query.1, bf16[512,512]{1,0:T(8,128)(2,1)} %w_key.1, ...), custom_call_target="tpu_custom_call" | custom-call | tf_op jit(solution)/shard_map/pallas_call | solution.py:605
  46.8 1.3 %copy.17 = bf16[16,128]{1,0:T(8,128)(2,1)} copy(bf16[16,128]{1,0:T(8,128)(2,1)} %shard_map.145) | data formatting | bytes 8192
where the time goes:
time: 48.3 us; the launch traced here: 48.1 us
  Pallas kernels  46.8 us (97%)
  local copies, waits for them, and re-layouts  1.28 us (3%)
    pallas_call x1, Pallas kernels, layer(): pl.pallas_call(functools.partial(fused, n_kv, n_tp), out_shape=jax.ShapeD...  46.8 us
    unnamed x1, local copies, waits for them, and re-layouts  1.28 us

commit v1 on v0

v1 whole, which is shorter than its diff:
```python
import functools

import jax
import jax.numpy as jnp
from jax import lax
from jax.experimental import pallas as pl
from jax.experimental.pallas import tpu as pltpu
from jax.sharding import PartitionSpec as P

norm_eps = 1e-06


def combined_all(value, axis, join):
    pieces = jax.tree.map(lambda part: lax.all_gather(part, axis), value)
    head = jax.tree.map(lambda part: part[0], pieces)
    tail = jax.tree.map(lambda part: part[1:], pieces)
    total, _ = lax.scan(lambda total, section: (join(total, section), None), head, tail)
    return total


def combine_parts(earlier, later):
    top = jnp.maximum(earlier[0], later[0])
    early_factor = jnp.exp(earlier[0] - top)
    late_factor = jnp.exp(later[0] - top)
    totals = earlier[1] * early_factor + later[1] * late_factor
    summed = earlier[2] * early_factor[..., None] + later[2] * late_factor[..., None]
    return (top, totals, summed, earlier[3] + later[3])


def channel_mix(residual, gain_mixer, w_up, w_down, kv_index):
    width = gain_mixer.shape[0]
    block_start = kv_index * w_up.shape[0]
    piece = lax.all_gather(residual, "tp", axis=1, tiled=True)
    piece_f = piece.astype(jnp.float32)
    gain_part = lax.dynamic_slice_in_dim(gain_mixer, block_start, piece.shape[1], 0).astype(
        jnp.float32
    )
    scaled = (piece_f * gain_part).astype(jnp.bfloat16)
    upward = jnp.dot(scaled, w_up, preferred_element_type=jnp.float32)
    upward, squares = (upward, jnp.sum(piece_f * piece_f, axis=-1))
    up_total, square_total = lax.psum((upward, squares), "kv")
    mixer_scale = lax.rsqrt(square_total / width + norm_eps)
    active = jax.nn.relu(mixer_scale[:, None] * up_total)
    hidden = (active * active).astype(jnp.bfloat16)
    down = jnp.dot(hidden, w_down, preferred_element_type=jnp.float32)
    return lax.psum_scatter(down, "tp", scatter_dimension=1, tiled=True)


def shards(
    tokens,
    gain_attn,
    w_query,
    w_key,
    w_value,
    w_forget,
    forget_bias,
    keys_cache,
    values_cache,
    gates_cache,
    lengths,
    w_out,
    gain_mixer,
    w_up,
    w_down,
):
    kv_index = lax.axis_index("kv")
    tp_index = lax.axis_index("tp")
    row_block = w_query.shape[0]
    heads_here = gates_cache.shape[1]
    width = gain_attn.shape[0]
    row_start = kv_index * row_block
    head_start = tp_index * heads_here
    block_raw = lax.all_gather(tokens, "tp", axis=1, tiled=True)
    block_f = block_raw.astype(jnp.float32)
    gain_block = lax.dynamic_slice_in_dim(gain_attn, row_start, row_block, 0).astype(jnp.float32)
    block = (block_f * gain_block).astype(jnp.bfloat16)
    forget_block = lax.dynamic_slice(w_forget, (row_start, head_start), (row_block, heads_here))
    part_query = jnp.dot(block, w_query, preferred_element_type=jnp.float32)
    part_key = jnp.dot(block, w_key, preferred_element_type=jnp.float32)
    part_value = jnp.dot(block, w_value, preferred_element_type=jnp.float32)
    part_gate = jnp.dot(block, forget_block, preferred_element_type=jnp.float32)
    part_squares = jnp.sum(block_f * block_f, axis=-1)
    sum_query, sum_key, sum_value, sum_gate, squares = lax.psum(
        (part_query, part_key, part_value, part_gate, part_squares), "kv"
    )
    attn_scale = lax.rsqrt(squares / width + norm_eps)[:, None]
    gate_logit = attn_scale * sum_gate
    query = (attn_scale * sum_query).astype(jnp.bfloat16)
    new_key = (attn_scale * sum_key).astype(jnp.bfloat16)
    new_value = (attn_scale * sum_value).astype(jnp.bfloat16)
    bias_here = lax.dynamic_slice_in_dim(forget_bias, head_start, heads_here, 0)
    forget_log = jax.nn.log_sigmoid(gate_logit + bias_here)
    seqs = tokens.shape[0]
    positions_here = keys_cache.shape[1]
    query_heads = query.reshape(seqs, heads_here, -1)
    head_size = query_heads.shape[-1]
    keys_heads = keys_cache.reshape(seqs, positions_here, heads_here, head_size)
    values_heads = values_cache.reshape(seqs, positions_here, heads_here, head_size)
    scores = jnp.einsum(
        "bhd,bphd->bhp", query_heads, keys_heads, preferred_element_type=jnp.float32
    )
    logits = scores * head_size ** (-0.5) - gates_cache
    positions = kv_index * positions_here + jnp.arange(positions_here, dtype=jnp.int32)
    valid = (positions[None, :] < lengths[:, None])[:, None, :]
    local_top = jnp.max(jnp.where(valid, logits, -1e30), axis=-1)
    weights = jnp.where(valid, jnp.exp(logits - local_top[..., None]), 0.0)
    local_total = jnp.sum(weights, axis=-1)
    local_sum = jnp.einsum(
        "bhp,bphd->bhd",
        weights.astype(jnp.bfloat16),
        values_heads,
        preferred_element_type=jnp.float32,
    )
    at_last = (positions[None, :] == lengths[:, None] - 1)[:, None, :]
    last_local = jnp.sum(jnp.where(at_last, gates_cache, 0.0), axis=-1)
    top, totals, summed, last_gate = combined_all(
        (local_top, local_total, local_sum, last_local), "kv", combine_parts
    )
    top = top + last_gate + forget_log
    own = jnp.sum(
        query_heads.astype(jnp.float32) * new_key.reshape(seqs, heads_here, -1).astype(jnp.float32),
        axis=-1,
    ) * head_size ** (-0.5)
    overall = jnp.maximum(top, own)
    cache_factor = jnp.exp(top - overall)
    own_weight = jnp.exp(own - overall)
    denominator = totals * cache_factor + own_weight
    numerator = summed * cache_factor[..., None] + own_weight[..., None] * new_value.reshape(
        seqs, heads_here, -1
    ).astype(jnp.float32)
    mixed = (numerator / denominator[..., None]).astype(jnp.bfloat16).reshape(seqs, -1)
    partial_value = jnp.dot(mixed, w_out, preferred_element_type=jnp.float32).astype(jnp.bfloat16)
    attended = lax.psum_scatter(partial_value, "tp", scatter_dimension=1, tiled=True).astype(
        jnp.float32
    )
    residual = (tokens.astype(jnp.float32) + attended).astype(jnp.bfloat16)
    mixer = channel_mix(residual, gain_mixer, w_up, w_down, kv_index)
    return (residual.astype(jnp.float32) + mixer).astype(jnp.bfloat16)


f32, bf16 = jnp.float32, jnp.bfloat16
LANES = 128


def spread_rows(rows, width):
    shape = (rows, width)
    return lax.broadcasted_iota(jnp.int32, shape, 0), lax.broadcasted_iota(jnp.int32, shape, 1)


def to_row(column):
    row, lane = spread_rows(column.shape[0], LANES)
    return jnp.sum(jnp.where(row == lane, column, 0.0), axis=0, keepdims=True)


def to_column(line, count):
    row, lane = spread_rows(count, LANES)
    return jnp.sum(jnp.where(row == lane, line, 0.0), axis=-1, keepdims=True)


def fused(
    n_kv,
    n_tp,
    tokens,
    gain_attn_any,
    forget_bias_any,
    lengths_any,
    gain_mixer_any,
    w_query,
    w_key,
    w_value,
    w_forget,
    keys_cache,
    values_cache,
    gates_cache,
    w_out,
    w_up,
    w_down,
    out,
    gain_attn,
    gain_mixer,
    forget_bias,
    lengths,
    wq,
    wk,
    wv,
    wf,
    keys,
    values,
    gates,
    wo,
    wu,
    wd,
    bias_t,
    tok_all,
    q_all,
    p_send,
    p_all,
    s_all,
    g_all,
    t_all,
    n_all,
    a_all,
    o_all,
    u_send,
    u_all,
    h_all,
    f_send,
    f_all,
    query,
    coef,
    res,
    load_sem,
    kv_out,
    kv_in,
    tp_out,
    tp_in,
    u_out,
    u_in,
    h_out,
    h_in,
):
    kv, tp = lax.axis_index("kv"), lax.axis_index("tp")
    seqs, piece = tok_all.shape[1:]
    rows, cols = wq.shape
    positions = keys.shape[1]
    heads = gates.shape[1]
    all_heads = wf.shape[0]
    size = cols // heads
    mine = seqs // n_kv
    width = gain_attn.shape[0]
    q_parts, q_rows = q_all.shape[1:3]
    a_parts, a_rows = a_all.shape[1:3]
    n_own, chunks = h_all.shape[:2]
    part = h_all.shape[3]
    first = n_kv // 4
    upper = kv // n_own
    is_owner = jnp.logical_and(kv >= first, kv < first + n_own)
    never = -3e38

    barrier = pltpu.get_barrier_semaphore()
    for j in range(1, n_tp):
        pl.semaphore_signal(
            barrier,
            inc=1,
            device_id=(kv, lax.rem(tp + j, n_tp)),
            device_id_type=pl.DeviceIdType.MESH,
        )
    turn = 2 * upper - 1

    def kv_peer(j):
        return lax.rem(kv + turn * j + n_kv, n_kv)

    for j in range(1, n_kv):
        pl.semaphore_signal(
            barrier,
            inc=1,
            device_id=(kv_peer(j), tp),
            device_id_type=pl.DeviceIdType.MESH,
        )

    row_at = pl.multiple_of(kv * rows, rows)
    sources = [
        (tokens, tok_all.at[tp]),
        (lengths_any, lengths),
        (gain_attn_any, gain_attn),
        (forget_bias_any, forget_bias),
        (gain_mixer_any, gain_mixer),
        (gates_cache, gates),
        (w_query, wq),
        (w_forget.at[:, pl.ds(row_at, rows)], wf),
        (w_key, wk),
        (w_value, wv),
        (keys_cache, keys),
        (values_cache, values),
        (w_out, wo),
        (w_up, wu),
        (w_down, wd),
    ]
    loads = [pltpu.make_async_copy(a, b, load_sem.at[i]) for i, (a, b) in enumerate(sources)]
    for load in loads:
        load.start()
    (
        ld_tok,
        ld_len,
        ld_ga,
        ld_bias,
        ld_gm,
        ld_gates,
        ld_q,
        ld_f,
        ld_k,
        ld_v,
        ld_keys,
        ld_values,
        ld_o,
        ld_u,
        ld_d,
    ) = loads

    def remote(source, target, out_sem, in_sem, device):
        return pltpu.make_async_remote_copy(
            src_ref=source,
            dst_ref=target,
            send_sem=out_sem,
            recv_sem=in_sem,
            device_id=device,
            device_id_type=pl.DeviceIdType.MESH,
        )

    pending = []

    def flush():
        for copy in pending:
            copy.wait_send()
        pending.clear()

    def start(copy):
        copy.start()
        pending.append(copy)

    def spread_kv(phase, slot):
        for j in range(1, n_kv):
            start(
                remote(
                    slot(kv),
                    slot(kv),
                    kv_out.at[phase, j],
                    kv_in.at[phase, kv],
                    (kv_peer(j), tp),
                )
            )

    def from_kv(phase, j, slot):
        peer = lax.rem(kv - turn * j + n_kv, n_kv)
        remote(
            slot(peer), slot(peer), kv_out.at[phase, j], kv_in.at[phase, peer], (peer, tp)
        ).wait_recv()

    def gather_kv(phase, slot):
        for j in range(1, n_kv):
            from_kv(phase, j, slot)

    def spread_tp(phase, slot):
        for j in range(1, n_tp):
            start(
                remote(
                    slot(tp),
                    slot(tp),
                    tp_out.at[phase, j],
                    tp_in.at[phase, tp],
                    (kv, lax.rem(tp + j, n_tp)),
                )
            )

    def gather_tp(phase, slot):
        for j in range(1, n_tp):
            peer = lax.rem(tp + n_tp - j, n_tp)
            remote(
                slot(peer), slot(peer), tp_out.at[phase, j], tp_in.at[phase, peer], (kv, peer)
            ).wait_recv()

    def total_of(read):
        total = read(0).astype(f32)
        for o in range(1, n_kv):
            total = total + read(o).astype(f32)
        return total

    ld_tok.wait()
    pl.semaphore_wait(barrier, n_kv + n_tp - 2)
    spread_tp(0, lambda t: tok_all.at[t])

    ld_len.wait()
    ld_ga.wait()
    ld_bias.wait()
    ld_gm.wait()
    ld_gates.wait()
    lane_seq = lax.broadcasted_iota(jnp.int32, (1, LANES), 1) // heads
    length_row = jnp.zeros((1, LANES), jnp.int32)
    for b in range(seqs):
        length_row = jnp.where(lane_seq == b, lengths[b], length_row)
    gates_t = jnp.transpose(gates[...].reshape(seqs * heads, positions))
    place = kv * positions + lax.broadcasted_iota(jnp.int32, (positions, LANES), 0)
    bias_t[...] = jnp.where(place < length_row, -gates_t, never)
    last_row = jnp.sum(jnp.where(place == length_row - 1, gates_t, 0.0), axis=0, keepdims=True)
    gain_a = gain_attn[pl.ds(row_at, rows)].astype(f32).reshape(1, rows)
    gain_m = gain_mixer[pl.ds(row_at, rows)].astype(f32).reshape(1, rows)

    gather_tp(0, lambda t: tok_all.at[t])
    tok = jnp.concatenate([tok_all[t] for t in range(n_tp)], axis=1).astype(f32)
    scaled = (tok * gain_a).astype(bf16)
    s_all[0, kv] = to_row(jnp.sum(tok * tok, axis=-1, keepdims=True))
    spread_kv(0, lambda o: s_all.at[0, o])
    ld_q.wait()
    q_part = jnp.dot(scaled, wq[...], preferred_element_type=f32).astype(bf16)
    for c in range(q_parts):
        q_all[kv, c] = q_part[c * q_rows : (c + 1) * q_rows]
    for c in range(q_parts):
        spread_kv(1 + c, lambda o, c=c: q_all.at[o, c])

    ld_k.wait()
    ld_v.wait()
    ld_f.wait()
    part_key = jnp.dot(scaled, wk[...], preferred_element_type=f32)
    part_value = jnp.dot(scaled, wv[...], preferred_element_type=f32)
    for o in range(n_kv):
        at = slice(o * mine, (o + 1) * mine)
        p_send[o, :, :cols] = part_key[at]
        p_send[o, :, cols:] = part_value[at]
    for j in range(1, n_kv):
        peer = kv_peer(j)
        start(
            remote(
                p_send.at[peer],
                p_all.at[kv],
                kv_out.at[P_PHASE, j],
                kv_in.at[P_PHASE, kv],
                (peer, tp),
            )
        )
    p_all[kv] = p_send[kv]

    part_gate = lax.dot_general(
        scaled, wf[...], (((1,), (1,)), ((), ())), preferred_element_type=f32
    )
    tall = jnp.concatenate(
        [part_gate, jnp.broadcast_to(forget_bias[...], (8, all_heads))], axis=0
    )
    head_lane = lax.broadcasted_iota(jnp.int32, tall.shape, 1) - tp * heads
    lane_head = lax.broadcasted_iota(jnp.int32, (1, LANES), 1) % heads
    wide = jnp.zeros((seqs + 8, LANES), f32)
    for h in range(heads):
        column = jnp.sum(jnp.where(head_lane == h, tall, 0.0), axis=-1, keepdims=True)
        wide = jnp.where(lane_head == h, column, wide)
    seq_row = lax.broadcasted_iota(jnp.int32, (seqs, LANES), 0)
    here = seq_row == lane_seq
    g_all[kv, 0:1, :] = jnp.sum(jnp.where(here, wide[:seqs], 0.0), axis=0, keepdims=True)
    g_all[kv, 1:2, :] = last_row
    spread_kv(G_PHASE, lambda o: g_all.at[o])
    bias_row = wide[seqs : seqs + 1]

    gather_kv(0, lambda o: s_all.at[0, o])
    squares = to_column(total_of(lambda o: s_all[0, o]), seqs)
    attn_scale = lax.rsqrt(squares / width + norm_eps)
    query[:, cols:] = jnp.broadcast_to(attn_scale, (seqs, LANES))
    own_block = (
        lax.broadcasted_iota(jnp.int32, (heads, cols), 0)
        == lax.broadcasted_iota(jnp.int32, (heads, cols), 1) // size
    )
    ld_keys.wait()
    scores = jnp.zeros((positions, LANES), f32)
    for c in range(q_parts):
        gather_kv(1 + c, lambda o, c=c: q_all.at[o, c])
        q_here = total_of(lambda o, c=c: q_all[o, c])
        q_here = (attn_scale[c * q_rows : (c + 1) * q_rows] * q_here).astype(bf16).astype(f32)
        query[c * q_rows : (c + 1) * q_rows, :cols] = q_here
        lefts, rights = [], []
        for r in range(q_rows):
            b = c * q_rows + r
            block = jnp.where(own_block, q_here[r : r + 1], 0.0)
            right = [jnp.zeros((b * heads, cols), f32)] if b else []
            right.append(block)
            if b + 1 < seqs:
                right.append(jnp.zeros(((seqs - b - 1) * heads, cols), f32))
            rights.append(jnp.concatenate(right, axis=0).astype(bf16))
            lefts.append(keys[b])
        scores = scores + lax.dot_general(
            jnp.concatenate(lefts, axis=1),
            jnp.concatenate(rights, axis=1),
            (((1,), (1,)), ((), ())),
            preferred_element_type=f32,
        )

    logits = scores * size ** (-0.5) + bias_t[...]
    top = jnp.maximum(jnp.max(logits, axis=0, keepdims=True), -1e30)
    weights = jnp.exp(logits - top)
    t_all[kv, 0:1, :] = top
    t_all[kv, 1:2, :] = jnp.sum(weights, axis=0, keepdims=True)
    spread_kv(T_PHASE, lambda o: t_all.at[o])
    weights = jnp.transpose(weights).astype(bf16)
    ld_values.wait()

    def attend(pair):
        left = weights[pair * 2 * heads : (pair + 1) * 2 * heads]
        found = []
        for r in range(2):
            summed = jnp.dot(left, values[2 * pair + r], preferred_element_type=f32)
            summed = jnp.where(own_block, summed[r * heads : (r + 1) * heads], 0.0)
            found.append(jnp.sum(summed, axis=0, keepdims=True))
        return found

    def own_token():
        gather_kv(P_PHASE, lambda o: p_all.at[o])
        gather_kv(G_PHASE, lambda o: g_all.at[o])
        scale_row = jnp.sum(jnp.where(here, attn_scale, 0.0), axis=0, keepdims=True)
        gate_sum = total_of(lambda o: g_all[o])
        gate_logit = scale_row * gate_sum[0:1] + bias_row
        forget_log = jnp.minimum(gate_logit, 0.0) - jnp.log1p(jnp.exp(-jnp.abs(gate_logit)))
        p_total = total_of(lambda o: p_all[o])
        own_rows = [query[pl.ds(kv * mine + r, 1), :] for r in range(mine)]
        own_query = jnp.concatenate(own_rows, axis=0)
        own_scale = own_query[:, cols : cols + 1]
        new_key = (own_scale * p_total[:, :cols]).astype(bf16).astype(f32)
        n_all[kv, :, :cols] = (own_scale * p_total[:, cols:]).astype(bf16).astype(f32)
        product = own_query[:, :cols] * new_key
        col_head = lax.broadcasted_iota(jnp.int32, (mine, cols), 1) // size
        own = jnp.full((mine, LANES), never, f32)
        own_seq = kv * mine + lax.broadcasted_iota(jnp.int32, (mine, LANES), 0)
        for h in range(heads):
            column = jnp.sum(jnp.where(col_head == h, product, 0.0), axis=-1, keepdims=True)
            at = jnp.logical_and(lane_head == h, lane_seq == own_seq)
            own = jnp.where(at, column * size ** (-0.5), own)
        own = own - jnp.where(lane_seq == own_seq, gate_sum[1:2] + forget_log, 0.0)
        n_all[kv, :, cols:] = own
        spread_kv(N_PHASE, lambda o: n_all.at[o])

    def weigh_parts():
        gather_kv(T_PHASE, lambda o: t_all.at[o])
        gather_kv(N_PHASE, lambda o: n_all.at[o])
        own = jnp.max(n_all[0, :, cols:], axis=0, keepdims=True)
        for o in range(1, n_kv):
            own = jnp.maximum(own, jnp.max(n_all[o, :, cols:], axis=0, keepdims=True))
        tops = [t_all[o, 0:1, :] for o in range(n_kv)] + [own]
        totals = [t_all[o, 1:2, :] for o in range(n_kv)] + [jnp.ones((1, LANES), f32)]
        overall = functools.reduce(jnp.maximum, tops)
        factors = [jnp.exp(one - overall) for one in tops]
        denominator = sum(one * total for one, total in zip(factors, totals))
        stack = jnp.concatenate(
            [jnp.where(here, one / denominator, 0.0) for one in factors], axis=0
        )
        high = stack.astype(bf16)
        low = (stack - high.astype(f32)).astype(bf16)
        lane = lax.broadcasted_iota(jnp.int32, (2 * LANES, cols), 0) % heads
        same = lane == lax.broadcasted_iota(jnp.int32, (2 * LANES, cols), 1) // size
        coef[...] = jnp.dot(
            jnp.concatenate([high, low], axis=1),
            jnp.where(same, 1.0, 0.0).astype(bf16),
            preferred_element_type=f32,
        )

    pairs_per = a_rows // 2
    for c in range(a_parts):
        found = []
        for i in range(pairs_per):
            found.extend(attend(c * pairs_per + i))
        a_all[kv, c] = jnp.concatenate(found, axis=0).astype(bf16)
        spread_kv(A_PHASE + c, lambda o, c=c: a_all.at[o, c])
        if c == 0:
            own_token()
    flush()
    weigh_parts()
    ld_o.wait()
    added = []
    new_values = jnp.concatenate([n_all[o, :, :cols] for o in range(n_kv)], axis=0)
    for c in range(a_parts):
        gather_kv(A_PHASE + c, lambda o, c=c: a_all.at[o, c])
        own_at = n_kv * seqs + c * a_rows
        mixed = coef[own_at : own_at + a_rows] * new_values[c * a_rows : (c + 1) * a_rows]
        for o in range(n_kv):
            at = o * seqs + c * a_rows
            mixed = mixed + coef[at : at + a_rows] * a_all[o, c].astype(f32)
        added.append(mixed)
    mixed = jnp.concatenate(added, axis=0).astype(bf16)
    o_all[tp] = jnp.dot(mixed, wo[...], preferred_element_type=f32).astype(bf16)
    spread_tp(1, lambda t: o_all.at[t])
    ld_u.wait()
    flush()
    gather_tp(1, lambda t: o_all.at[t])
    attended = o_all[0].astype(f32)
    for t in range(1, n_tp):
        attended = attended + o_all[t].astype(f32)
    residual = (tok + attended).astype(bf16).astype(f32)
    for t in range(n_tp):
        res[t] = residual[:, t * piece : (t + 1) * piece]
    scaled_mid = (residual * gain_m).astype(bf16)

    def owner_at(j):
        near = (n_own // 2 + j) % n_own
        return near + upper * (n_own - 1 - 2 * near)

    def elsewhere(m, act):
        pl.when(first + m != kv)(act)

    s_all[1, kv] = to_row(jnp.sum(residual * residual, axis=-1, keepdims=True))

    def square_copy(m):
        return remote(
            s_all.at[1, kv],
            s_all.at[1, kv],
            u_out.at[chunks, m],
            u_in.at[chunks, kv],
            (first + m, tp),
        )

    def up_copy(m, c):
        return remote(
            u_send.at[m, c], u_all.at[kv, c], u_out.at[c, m], u_in.at[c, kv], (first + m, tp)
        )

    for j in range(n_own):
        m = owner_at(j)
        elsewhere(m, lambda m=m: square_copy(m).start())
    for c in range(chunks):
        for j in range(n_own):
            m = owner_at(j)
            at = pl.multiple_of((m * chunks + c) * part, part)
            u_send[m, c] = jnp.dot(
                scaled_mid, wu[:, pl.ds(at, part)], preferred_element_type=f32
            ).astype(bf16)
            elsewhere(m, lambda m=m, c=c: up_copy(m, c).start())

    own_m = kv - first

    def hidden_copy(c, j):
        return remote(
            h_all.at[own_m, c],
            h_all.at[own_m, c],
            h_out.at[c, j],
            h_in.at[c, own_m],
            (kv_peer(j), tp),
        )


    @pl.when(is_owner)
    def _():
        for j in range(1, n_kv):
            peer = lax.rem(kv - turn * j + n_kv, n_kv)
            remote(
                s_all.at[1, peer],
                s_all.at[1, peer],
                u_out.at[chunks, 0],
                u_in.at[chunks, peer],
                (peer, tp),
            ).wait_recv()
        squares = to_column(total_of(lambda o: s_all[1, o]), seqs)
        mixer_scale = lax.rsqrt(squares / width + norm_eps)
        for c in range(chunks):
            total = u_send[own_m, c].astype(f32)
            for j in range(1, n_kv):
                peer = lax.rem(kv - turn * j + n_kv, n_kv)
                remote(
                    u_all.at[peer, c],
                    u_all.at[peer, c],
                    u_out.at[c, 0],
                    u_in.at[c, peer],
                    (peer, tp),
                ).wait_recv()
                total = total + u_all[peer, c].astype(f32)
            active = jnp.maximum(mixer_scale * total, 0.0)
            h_all[own_m, c] = (active * active).astype(bf16)
            for j in range(1, n_kv):
                hidden_copy(c, j).start()

    ld_d.wait()
    for c in range(chunks):
        for j in range(n_own):
            m = owner_at(j)
            elsewhere(m, lambda m=m, c=c: up_copy(m, c).wait_send())
    for j in range(n_own):
        m = owner_at(j)
        elsewhere(m, lambda m=m: square_copy(m).wait_send())

    down = jnp.zeros((seqs, rows), f32)
    for c in range(chunks):
        for j in reversed(range(n_own)):
            m = owner_at(j)

            def arrive(m=m, c=c):
                remote(
                    h_all.at[m, c],
                    h_all.at[m, c],
                    h_out.at[c, 0],
                    h_in.at[c, m],
                    (first + m, tp),
                ).wait_recv()

            elsewhere(m, arrive)
            at = pl.multiple_of((m * chunks + c) * part, part)
            down = down + jnp.dot(
                h_all[m, c], wd[pl.ds(at, part), :], preferred_element_type=f32
            )
    for t in range(n_tp):
        f_send[t] = down[:, t * piece : (t + 1) * piece].astype(bf16)
    for j in range(1, n_tp):
        peer = lax.rem(tp + j, n_tp)
        start(
            remote(
                f_send.at[peer], f_all.at[tp], tp_out.at[2, j], tp_in.at[2, tp], (kv, peer)
            )
        )
    f_all[tp] = f_send[tp]

    @pl.when(is_owner)
    def _():
        for c in range(chunks):
            for j in range(1, n_kv):
                hidden_copy(c, j).wait_send()

    flush()
    gather_tp(2, lambda t: f_all.at[t])
    mixer = f_all[0].astype(f32)
    for t in range(1, n_tp):
        mixer = mixer + f_all[t].astype(f32)
    out[...] = (res[tp] + mixer).astype(bf16)


Q_PARTS = 2
A_PARTS = 2
CHUNKS = 2
P_PHASE = 1 + Q_PARTS
G_PHASE = P_PHASE + 1
T_PHASE = G_PHASE + 1
N_PHASE = T_PHASE + 1
A_PHASE = N_PHASE + 1
PHASES = A_PHASE + A_PARTS


def layer(n_kv, n_tp, *arrays):
    (
        tokens,
        gain_attn,
        w_query,
        w_key,
        w_value,
        w_forget,
        forget_bias,
        keys_cache,
        values_cache,
        gates_cache,
        lengths,
        w_out,
        gain_mixer,
        w_up,
        w_down,
    ) = arrays
    seqs, piece = tokens.shape
    rows, cols = w_query.shape
    positions = keys_cache.shape[1]
    heads = gates_cache.shape[1]
    all_heads = w_forget.shape[1]
    n_own = n_kv // 2
    part = w_up.shape[1] // max(n_own * CHUNKS, 1)
    fits = (
        n_kv % 4 == 0
        and n_tp > 1
        and seqs % n_kv == 0
        and seqs * heads == LANES
        and heads % 8 == 0
        and seqs % (8 * max(Q_PARTS, A_PARTS)) == 0
        and piece % LANES == 0
        and cols % LANES == 0
        and positions % LANES == 0
        and part % LANES == 0
        and w_up.shape[1] == part * n_own * CHUNKS
        and all_heads <= LANES
        and w_out.shape == (cols, rows)
        and rows == n_tp * piece
    )
    if not fits:
        return shards(*arrays)
    mine = seqs // n_kv
    vmem = pl.BlockSpec(memory_space=pltpu.VMEM)
    anywhere = pl.BlockSpec(memory_space=pl.ANY)
    bias = forget_bias.reshape(1, -1)

    def like(x):
        return pltpu.VMEM(x.shape, x.dtype)

    return pl.pallas_call(
        functools.partial(fused, n_kv, n_tp),
        out_shape=jax.ShapeDtypeStruct((seqs, piece), bf16),
        in_specs=[anywhere] * 15,
        out_specs=vmem,
        scratch_shapes=[
            like(gain_attn),
            like(gain_mixer),
            like(bias),
            pltpu.SMEM(lengths.shape, lengths.dtype),
            like(w_query),
            like(w_key),
            like(w_value),
            pltpu.VMEM((all_heads, rows), bf16),
            like(keys_cache),
            like(values_cache),
            like(gates_cache),
            like(w_out),
            like(w_up),
            like(w_down),
            pltpu.VMEM((positions, LANES), f32),
            pltpu.VMEM((n_tp, seqs, piece), bf16),
            pltpu.VMEM((n_kv, Q_PARTS, seqs // Q_PARTS, cols), bf16),
            pltpu.VMEM((n_kv, mine, 2 * cols), f32),
            pltpu.VMEM((n_kv, mine, 2 * cols), f32),
            pltpu.VMEM((2, n_kv, 1, LANES), f32),
            pltpu.VMEM((n_kv, 2, LANES), f32),
            pltpu.VMEM((n_kv, 2, LANES), f32),
            pltpu.VMEM((n_kv, mine, cols + LANES), f32),
            pltpu.VMEM((n_kv, A_PARTS, seqs // A_PARTS, cols), bf16),
            pltpu.VMEM((n_tp, seqs, rows), bf16),
            pltpu.VMEM((n_own, CHUNKS, seqs, part), bf16),
            pltpu.VMEM((n_kv, CHUNKS, seqs, part), bf16),
            pltpu.VMEM((n_own, CHUNKS, seqs, part), bf16),
            pltpu.VMEM((n_tp, seqs, piece), bf16),
            pltpu.VMEM((n_tp, seqs, piece), bf16),
            pltpu.VMEM((seqs, cols + LANES), f32),
            pltpu.VMEM(((n_kv + 1) * seqs, cols), f32),
            pltpu.VMEM((n_tp, seqs, piece), f32),
            pltpu.SemaphoreType.DMA((15,)),
            pltpu.SemaphoreType.DMA((PHASES, n_kv)),
            pltpu.SemaphoreType.DMA((PHASES, n_kv)),
            pltpu.SemaphoreType.DMA((3, n_tp)),
            pltpu.SemaphoreType.DMA((3, n_tp)),
            pltpu.SemaphoreType.DMA((CHUNKS + 1, n_own)),
            pltpu.SemaphoreType.DMA((CHUNKS + 1, n_kv)),
            pltpu.SemaphoreType.DMA((CHUNKS, n_kv)),
            pltpu.SemaphoreType.DMA((CHUNKS, n_own)),
        ],
        compiler_params=pltpu.CompilerParams(
            collective_id=0, has_side_effects=True, vmem_limit_bytes=VMEM_LIMIT
        ),
    )(
        tokens,
        gain_attn,
        bias,
        lengths,
        gain_mixer,
        w_query,
        w_key,
        w_value,
        w_forget.T,
        keys_cache,
        values_cache,
        gates_cache,
        w_out,
        w_up,
        w_down,
    )


VMEM_LIMIT = 60 * 1024 * 1024


def solution(mesh):
    return jax.shard_map(
        functools.partial(layer, mesh.shape["kv"], mesh.shape["tp"]),
        mesh=mesh,
        in_specs=(
            P(None, ("kv", "tp")),
            P(),
            P("kv", "tp"),
            P("kv", "tp"),
            P("kv", "tp"),
            P(),
            P(),
            P(None, "kv", "tp"),
            P(None, "kv", "tp"),
            P(None, "tp", "kv"),
            P(),
            P("tp", "kv"),
            P(),
            P("kv", "tp"),
            P("tp", "kv"),
        ),
        out_specs=P(None, ("kv", "tp")),
        check_vma=False,
    )
```

time: 48.3 us -> 46.6 us (0.965)
  Pallas kernels: 46.8 us -> 45.1 us
    pallas_call x1, Pallas kernels: 46.8 us -> 45.1 us  [layer(): pl.pallas_call(functools.partial(fused, n_kv, n_tp), out_shape=jax.ShapeD...]
where the time goes in v1:
time: 46.6 us; the launch traced here: 46.4 us
  Pallas kernels  45.1 us (97%)
  local copies, waits for them, and re-layouts  1.28 us (3%)
    pallas_call x1, Pallas kernels, layer(): pl.pallas_call(functools.partial(fused, n_kv, n_tp), out_shape=jax.ShapeD...  45.1 us
    unnamed x1, local copies, waits for them, and re-layouts  1.28 us

profile of v1, /device:TPU:0, one launch (start us, length us, event | category | flops | bytes accessed | tf_op | source)
XLA Modules:
  0.0 46.4 jit_solution(17688438240887856311)
XLA Ops:
  0.0 45.1 %shard_map.145 = bf16[16,128]{1,0:T(8,128)(2,1)} custom-call(bf16[16,128]{1,0:T(8,128)(2,1)} %tokens.1, bf16[4096]{0:T(1024)(128)(2,1)} %gain_attn_any.1, f32[1,32]{1,0:T(1,128)} %bitcast.3, s32[16]{0:T(128)} %lengths_any.1, bf16[4096]{0:T(1024)(128)(2,1)} %gain_mixer_any.1, bf16[512,512]{1,0:T(8,128)(2,1)} %w_query.1, bf16[512,512]{1,0:T(8,128)(2,1)} %w_key.1, ...), custom_call_target="tpu_custom_call" | custom-call | tf_op jit(solution)/shard_map/pallas_call | solution.py:768
  45.1 1.3 %copy.17 = bf16[16,128]{1,0:T(8,128)(2,1)} copy(bf16[16,128]{1,0:T(8,128)(2,1)} %shard_map.145) | data formatting | bytes 8192

commit v2 on v1

--- a/solution.py
+++ b/solution.py
@@ -190,7 +190,9 @@
     wo,
     wu,
     wd,
-    bias_t,
+    bias,
+    logits,
+    weights,
     tok_all,
     q_all,
     p_send,
@@ -208,6 +210,7 @@
     f_all,
     query,
     coef,
+    mid,
     res,
     load_sem,
     kv_out,
@@ -232,8 +235,8 @@
     a_parts, a_rows = a_all.shape[1:3]
     n_own, chunks = h_all.shape[:2]
     part = h_all.shape[3]
-    first = n_kv // 4
-    upper = kv // n_own
+    first = (n_kv - n_own) // 2
+    upper = kv // (n_kv // 2)
     is_owner = jnp.logical_and(kv >= first, kv < first + n_own)
     never = -3e38
 
@@ -310,54 +313,36 @@
     pending = []
 
     def flush():
-        for copy in pending:
-            copy.wait_send()
+        for many, sem in pending:
+            remote(many, many, sem, sem, (kv_peer(1), tp)).wait_send()
         pending.clear()
 
-    def start(copy):
-        copy.start()
-        pending.append(copy)
+    def landed(many, sem):
+        remote(many, many, sem, sem, (kv_peer(1), tp)).wait_recv()
 
     def spread_kv(phase, slot):
         for j in range(1, n_kv):
-            start(
-                remote(
-                    slot(kv),
-                    slot(kv),
-                    kv_out.at[phase, j],
-                    kv_in.at[phase, kv],
-                    (kv_peer(j), tp),
-                )
-            )
-
-    def from_kv(phase, j, slot):
-        peer = lax.rem(kv - turn * j + n_kv, n_kv)
-        remote(
-            slot(peer), slot(peer), kv_out.at[phase, j], kv_in.at[phase, peer], (peer, tp)
-        ).wait_recv()
+            remote(
+                slot(kv), slot(kv), kv_out.at[phase], kv_in.at[phase], (kv_peer(j), tp)
+            ).start()
+        pending.append((slot(pl.ds(0, n_kv - 1)), kv_out.at[phase]))
 
     def gather_kv(phase, slot):
-        for j in range(1, n_kv):
-            from_kv(phase, j, slot)
+        landed(slot(pl.ds(0, n_kv - 1)), kv_in.at[phase])
 
     def spread_tp(phase, slot):
         for j in range(1, n_tp):
-            start(
-                remote(
-                    slot(tp),
-                    slot(tp),
-                    tp_out.at[phase, j],
-                    tp_in.at[phase, tp],
-                    (kv, lax.rem(tp + j, n_tp)),
-                )
-            )
+            remote(
+                slot(tp),
+                slot(tp),
+                tp_out.at[phase],
+                tp_in.at[phase],
+                (kv, lax.rem(tp + j, n_tp)),
+            ).start()
+        pending.append((slot(pl.ds(0, n_tp - 1)), tp_out.at[phase]))
 
     def gather_tp(phase, slot):
-        for j in range(1, n_tp):
-            peer = lax.rem(tp + n_tp - j, n_tp)
-            remote(
-                slot(peer), slot(peer), tp_out.at[phase, j], tp_in.at[phase, peer], (kv, peer)
-            ).wait_recv()
+        landed(slot(pl.ds(0, n_tp - 1)), tp_in.at[phase])
 
     def total_of(read):
         total = read(0).astype(f32)
@@ -375,25 +360,27 @@
     ld_gm.wait()
     ld_gates.wait()
     lane_seq = lax.broadcasted_iota(jnp.int32, (1, LANES), 1) // heads
-    length_row = jnp.zeros((1, LANES), jnp.int32)
+    place = kv * positions + lax.broadcasted_iota(jnp.int32, (heads, positions), 1)
+    lasts = []
     for b in range(seqs):
-        length_row = jnp.where(lane_seq == b, lengths[b], length_row)
-    gates_t = jnp.transpose(gates[...].reshape(seqs * heads, positions))
-    place = kv * positions + lax.broadcasted_iota(jnp.int32, (positions, LANES), 0)
-    bias_t[...] = jnp.where(place < length_row, -gates_t, never)
-    last_row = jnp.sum(jnp.where(place == length_row - 1, gates_t, 0.0), axis=0, keepdims=True)
+        gate = gates[b]
+        length = lengths[b]
+        bias[b * heads : (b + 1) * heads] = jnp.where(place < length, -gate, never)
+        last = jnp.where(place == length - 1, gate, 0.0)
+        lasts.append(jnp.sum(last, axis=-1, keepdims=True))
+    last_row = to_row(jnp.concatenate(lasts, axis=0))
     gain_a = gain_attn[pl.ds(row_at, rows)].astype(f32).reshape(1, rows)
     gain_m = gain_mixer[pl.ds(row_at, rows)].astype(f32).reshape(1, rows)
 
     gather_tp(0, lambda t: tok_all.at[t])
     tok = jnp.concatenate([tok_all[t] for t in range(n_tp)], axis=1).astype(f32)
     scaled = (tok * gain_a).astype(bf16)
-    s_all[0, kv] = to_row(jnp.sum(tok * tok, axis=-1, keepdims=True))
-    spread_kv(0, lambda o: s_all.at[0, o])
     ld_q.wait()
     q_part = jnp.dot(scaled, wq[...], preferred_element_type=f32).astype(bf16)
+    s_all[0, kv] = to_row(jnp.sum(tok * tok, axis=-1, keepdims=True))
     for c in range(q_parts):
         q_all[kv, c] = q_part[c * q_rows : (c + 1) * q_rows]
+    spread_kv(0, lambda o: s_all.at[0, o])
     for c in range(q_parts):
         spread_kv(1 + c, lambda o, c=c: q_all.at[o, c])
 
@@ -408,15 +395,10 @@
         p_send[o, :, cols:] = part_value[at]
     for j in range(1, n_kv):
         peer = kv_peer(j)
-        start(
-            remote(
-                p_send.at[peer],
-                p_all.at[kv],
-                kv_out.at[P_PHASE, j],
-                kv_in.at[P_PHASE, kv],
-                (peer, tp),
-            )
-        )
+        remote(
+            p_send.at[peer], p_all.at[kv], kv_out.at[P_PHASE], kv_in.at[P_PHASE], (peer, tp)
+        ).start()
+    pending.append((p_send.at[pl.ds(0, n_kv - 1)], kv_out.at[P_PHASE]))
     p_all[kv] = p_send[kv]
 
     part_gate = lax.dot_general(
@@ -447,36 +429,28 @@
         == lax.broadcasted_iota(jnp.int32, (heads, cols), 1) // size
     )
     ld_keys.wait()
-    scores = jnp.zeros((positions, LANES), f32)
     for c in range(q_parts):
         gather_kv(1 + c, lambda o, c=c: q_all.at[o, c])
         q_here = total_of(lambda o, c=c: q_all[o, c])
         q_here = (attn_scale[c * q_rows : (c + 1) * q_rows] * q_here).astype(bf16).astype(f32)
         query[c * q_rows : (c + 1) * q_rows, :cols] = q_here
-        lefts, rights = [], []
-        for r in range(q_rows):
-            b = c * q_rows + r
-            block = jnp.where(own_block, q_here[r : r + 1], 0.0)
-            right = [jnp.zeros((b * heads, cols), f32)] if b else []
-            right.append(block)
-            if b + 1 < seqs:
-                right.append(jnp.zeros(((seqs - b - 1) * heads, cols), f32))
-            rights.append(jnp.concatenate(right, axis=0).astype(bf16))
-            lefts.append(keys[b])
-        scores = scores + lax.dot_general(
-            jnp.concatenate(lefts, axis=1),
-            jnp.concatenate(rights, axis=1),
-            (((1,), (1,)), ((), ())),
-            preferred_element_type=f32,
-        )
-
-    logits = scores * size ** (-0.5) + bias_t[...]
-    top = jnp.maximum(jnp.max(logits, axis=0, keepdims=True), -1e30)
-    weights = jnp.exp(logits - top)
-    t_all[kv, 0:1, :] = top
-    t_all[kv, 1:2, :] = jnp.sum(weights, axis=0, keepdims=True)
+        for r in range(0, q_rows, 2):
+            pair = [jnp.where(own_block, q_here[r + i : r + i + 1], 0.0) for i in range(2)]
+            pair = jnp.concatenate(pair, axis=0).astype(bf16)
+            for i in range(2):
+                b = c * q_rows + r + i
+                scores = lax.dot_general(
+                    pair, keys[b], (((1,), (1,)), ((), ())), preferred_element_type=f32
+                )
+                logits[b * heads : (b + 1) * heads] = scores[i * heads : (i + 1) * heads]
+
+    scores = logits[...] * size ** (-0.5) + bias[...]
+    top = jnp.maximum(jnp.max(scores, axis=-1, keepdims=True), -1e30)
+    spread = jnp.exp(scores - top)
+    weights[...] = spread.astype(bf16)
+    t_all[kv, 0:1, :] = to_row(top)
+    t_all[kv, 1:2, :] = to_row(jnp.sum(spread, axis=-1, keepdims=True))
     spread_kv(T_PHASE, lambda o: t_all.at[o])
-    weights = jnp.transpose(weights).astype(bf16)
     ld_values.wait()
 
     def attend(pair):
@@ -537,6 +511,7 @@
             preferred_element_type=f32,
         )
 
+    own_token()
     pairs_per = a_rows // 2
     for c in range(a_parts):
         found = []
@@ -544,8 +519,6 @@
             found.extend(attend(c * pairs_per + i))
         a_all[kv, c] = jnp.concatenate(found, axis=0).astype(bf16)
         spread_kv(A_PHASE + c, lambda o, c=c: a_all.at[o, c])
-        if c == 0:
-            own_token()
     flush()
     weigh_parts()
     ld_o.wait()
@@ -571,130 +544,100 @@
     residual = (tok + attended).astype(bf16).astype(f32)
     for t in range(n_tp):
         res[t] = residual[:, t * piece : (t + 1) * piece]
-    scaled_mid = (residual * gain_m).astype(bf16)
-
-    def owner_at(j):
-        near = (n_own // 2 + j) % n_own
-        return near + upper * (n_own - 1 - 2 * near)
-
-    def elsewhere(m, act):
-        pl.when(first + m != kv)(act)
-
+    mid[...] = (residual * gain_m).astype(bf16)
     s_all[1, kv] = to_row(jnp.sum(residual * residual, axis=-1, keepdims=True))
-
-    def square_copy(m):
-        return remote(
-            s_all.at[1, kv],
-            s_all.at[1, kv],
-            u_out.at[chunks, m],
-            u_in.at[chunks, kv],
-            (first + m, tp),
-        )
-
-    def up_copy(m, c):
-        return remote(
-            u_send.at[m, c], u_all.at[kv, c], u_out.at[c, m], u_in.at[c, kv], (first + m, tp)
-        )
-
-    for j in range(n_own):
-        m = owner_at(j)
-        elsewhere(m, lambda m=m: square_copy(m).start())
-    for c in range(chunks):
-        for j in range(n_own):
-            m = owner_at(j)
+    own_m = kv - first
+
+    def mixer_part(owner):
+        if not owner:
+            order = [(n_own // 2 + j) % n_own for j in range(n_own)]
+            targets = [near + upper * (n_own - 1 - 2 * near) for near in order]
+        elif n_own == n_kv:
+            targets = [kv_peer(j) for j in range(1, n_kv)]
+        else:
+            order = [n_own // 2, *range(n_own // 2 + 1, n_own), *range(1, n_own // 2)]
+            targets = [lax.rem(own_m + j, n_own) for j in order]
+        count = len(targets)
+        for m in targets:
+            remote(
+                s_all.at[1, kv],
+                s_all.at[1, kv],
+                u_out.at[chunks],
+                u_in.at[chunks],
+                (first + m, tp),
+            ).start()
+
+        def up_piece(m, c):
             at = pl.multiple_of((m * chunks + c) * part, part)
-            u_send[m, c] = jnp.dot(
-                scaled_mid, wu[:, pl.ds(at, part)], preferred_element_type=f32
+            u_send[c, m] = jnp.dot(
+                mid[...], wu[:, pl.ds(at, part)], preferred_element_type=f32
             ).astype(bf16)
-            elsewhere(m, lambda m=m, c=c: up_copy(m, c).start())
-
-    own_m = kv - first
-
-    def hidden_copy(c, j):
-        return remote(
-            h_all.at[own_m, c],
-            h_all.at[own_m, c],
-            h_out.at[c, j],
-            h_in.at[c, own_m],
-            (kv_peer(j), tp),
-        )
-
-
-    @pl.when(is_owner)
-    def _():
-        for j in range(1, n_kv):
-            peer = lax.rem(kv - turn * j + n_kv, n_kv)
+
+        for c in range(chunks):
+            for m in targets:
+                up_piece(m, c)
+            for m in targets:
+                remote(
+                    u_send.at[c, m], u_all.at[c, kv], u_out.at[c], u_in.at[c], (first + m, tp)
+                ).start()
+        own_order = []
+        if owner:
+            for c in range(chunks):
+                up_piece(own_m, c)
+            landed(s_all.at[1, pl.ds(0, n_kv - 1)], u_in.at[chunks])
+            squares = to_column(total_of(lambda o: s_all[1, o]), seqs)
+            mixer_scale = lax.rsqrt(squares / width + norm_eps)
+            for c in range(chunks):
+                u_all[c, kv] = u_send[c, own_m]
+                landed(u_all.at[c, pl.ds(0, n_kv - 1)], u_in.at[c])
+                active = jnp.maximum(mixer_scale * total_of(lambda o, c=c: u_all[c, o]), 0.0)
+                h_all[own_m, c] = (active * active).astype(bf16)
+                for j in range(1, n_kv):
+                    remote(
+                        h_all.at[own_m, c],
+                        h_all.at[own_m, c],
+                        h_out.at[c],
+                        h_in.at[c, own_m],
+                        (kv_peer(j), tp),
+                    ).start()
+                own_order.append((c, own_m))
+
+        def down_piece(m, c):
+            at = pl.multiple_of((m * chunks + c) * part, part)
+            return jnp.dot(h_all[m, c], wd[pl.ds(at, part), :], preferred_element_type=f32)
+
+        ld_d.wait()
+        for c in range(chunks):
+            many = u_send.at[c, pl.ds(0, count)]
+            remote(many, many, u_out.at[c], u_out.at[c], (kv_peer(1), tp)).wait_send()
+        many = s_all.at[1, pl.ds(0, count)]
+        remote(many, many, u_out.at[chunks], u_out.at[chunks], (kv_peer(1), tp)).wait_send()
+        down = jnp.zeros((seqs, rows), f32)
+        for c, m in own_order:
+            down = down + down_piece(m, c)
+        for c in range(chunks):
+            for m in reversed(targets):
+                landed(h_all.at[m, c], h_in.at[c, m])
+                down = down + down_piece(m, c)
+        for t in range(n_tp):
+            f_send[t] = down[:, t * piece : (t + 1) * piece].astype(bf16)
+        for j in range(1, n_tp):
+            peer = lax.rem(tp + j, n_tp)
             remote(
-                s_all.at[1, peer],
-                s_all.at[1, peer],
-                u_out.at[chunks, 0],
-                u_in.at[chunks, peer],
-                (peer, tp),
-            ).wait_recv()
-        squares = to_column(total_of(lambda o: s_all[1, o]), seqs)
-        mixer_scale = lax.rsqrt(squares / width + norm_eps)
-        for c in range(chunks):
-            total = u_send[own_m, c].astype(f32)
-            for j in range(1, n_kv):
-                peer = lax.rem(kv - turn * j + n_kv, n_kv)
-                remote(
-                    u_all.at[peer, c],
-                    u_all.at[peer, c],
-                    u_out.at[c, 0],
-                    u_in.at[c, peer],
-                    (peer, tp),
-                ).wait_recv()
-                total = total + u_all[peer, c].astype(f32)
-            active = jnp.maximum(mixer_scale * total, 0.0)
-            h_all[own_m, c] = (active * active).astype(bf16)
-            for j in range(1, n_kv):
-                hidden_copy(c, j).start()
-
-    ld_d.wait()
-    for c in range(chunks):
-        for j in range(n_own):
-            m = owner_at(j)
-            elsewhere(m, lambda m=m, c=c: up_copy(m, c).wait_send())
-    for j in range(n_own):
-        m = owner_at(j)
-        elsewhere(m, lambda m=m: square_copy(m).wait_send())
-
-    down = jnp.zeros((seqs, rows), f32)
-    for c in range(chunks):
-        for j in reversed(range(n_own)):
-            m = owner_at(j)
-
-            def arrive(m=m, c=c):
-                remote(
-                    h_all.at[m, c],
-                    h_all.at[m, c],
-                    h_out.at[c, 0],
-                    h_in.at[c, m],
-                    (first + m, tp),
-                ).wait_recv()
-
-            elsewhere(m, arrive)
-            at = pl.multiple_of((m * chunks + c) * part, part)
-            down = down + jnp.dot(
-                h_all[m, c], wd[pl.ds(at, part), :], preferred_element_type=f32
-            )
-    for t in range(n_tp):
-        f_send[t] = down[:, t * piece : (t + 1) * piece].astype(bf16)
-    for j in range(1, n_tp):
-        peer = lax.rem(tp + j, n_tp)
-        start(
-            remote(
-                f_send.at[peer], f_all.at[tp], tp_out.at[2, j], tp_in.at[2, tp], (kv, peer)
-            )
-        )
-    f_all[tp] = f_send[tp]
-
-    @pl.when(is_owner)
-    def _():
-        for c in range(chunks):
-            for j in range(1, n_kv):
-                hidden_copy(c, j).wait_send()
-
+                f_send.at[peer], f_all.at[tp], tp_out.at[2], tp_in.at[2], (kv, peer)
+            ).start()
+        f_all[tp] = f_send[tp]
+        if owner:
+            for c in range(chunks):
+                many = u_all.at[c, pl.ds(0, n_kv - 1)]
+                remote(many, many, h_out.at[c], h_out.at[c], (kv_peer(1), tp)).wait_send()
+
+    if n_own == n_kv:
+        mixer_part(True)
+    else:
+        pl.when(is_owner)(lambda: mixer_part(True))
+        pl.when(jnp.logical_not(is_owner))(lambda: mixer_part(False))
+    pending.append((f_send.at[pl.ds(0, n_tp - 1)], tp_out.at[2]))
     flush()
     gather_tp(2, lambda t: f_all.at[t])
     mixer = f_all[0].astype(f32)
@@ -706,6 +649,7 @@
 Q_PARTS = 2
 A_PARTS = 2
 CHUNKS = 2
+OWNERS = 2
 P_PHASE = 1 + Q_PARTS
 G_PHASE = P_PHASE + 1
 T_PHASE = G_PHASE + 1
@@ -737,7 +681,7 @@
     positions = keys_cache.shape[1]
     heads = gates_cache.shape[1]
     all_heads = w_forget.shape[1]
-    n_own = n_kv // 2
+    n_own = n_kv // OWNERS
     part = w_up.shape[1] // max(n_own * CHUNKS, 1)
     fits = (
         n_kv % 4 == 0
@@ -785,7 +729,9 @@
             like(w_out),
             like(w_up),
             like(w_down),
-            pltpu.VMEM((positions, LANES), f32),
+            pltpu.VMEM((seqs * heads, positions), f32),
+            pltpu.VMEM((seqs * heads, positions), f32),
+            pltpu.VMEM((seqs * heads, positions), bf16),
             pltpu.VMEM((n_tp, seqs, piece), bf16),
             pltpu.VMEM((n_kv, Q_PARTS, seqs // Q_PARTS, cols), bf16),
             pltpu.VMEM((n_kv, mine, 2 * cols), f32),
@@ -796,22 +742,23 @@
             pltpu.VMEM((n_kv, mine, cols + LANES), f32),
             pltpu.VMEM((n_kv, A_PARTS, seqs // A_PARTS, cols), bf16),
             pltpu.VMEM((n_tp, seqs, rows), bf16),
-            pltpu.VMEM((n_own, CHUNKS, seqs, part), bf16),
-            pltpu.VMEM((n_kv, CHUNKS, seqs, part), bf16),
+            pltpu.VMEM((CHUNKS, n_own, seqs, part), bf16),
+            pltpu.VMEM((CHUNKS, n_kv, seqs, part), bf16),
             pltpu.VMEM((n_own, CHUNKS, seqs, part), bf16),
             pltpu.VMEM((n_tp, seqs, piece), bf16),
             pltpu.VMEM((n_tp, seqs, piece), bf16),
             pltpu.VMEM((seqs, cols + LANES), f32),
             pltpu.VMEM(((n_kv + 1) * seqs, cols), f32),
+            pltpu.VMEM((seqs, rows), bf16),
             pltpu.VMEM((n_tp, seqs, piece), f32),
             pltpu.SemaphoreType.DMA((15,)),
-            pltpu.SemaphoreType.DMA((PHASES, n_kv)),
-            pltpu.SemaphoreType.DMA((PHASES, n_kv)),
-            pltpu.SemaphoreType.DMA((3, n_tp)),
-            pltpu.SemaphoreType.DMA((3, n_tp)),
-            pltpu.SemaphoreType.DMA((CHUNKS + 1, n_own)),
-            pltpu.SemaphoreType.DMA((CHUNKS + 1, n_kv)),
-            pltpu.SemaphoreType.DMA((CHUNKS, n_kv)),
+            pltpu.SemaphoreType.DMA((PHASES,)),
+            pltpu.SemaphoreType.DMA((PHASES,)),
+            pltpu.SemaphoreType.DMA((3,)),
+            pltpu.SemaphoreType.DMA((3,)),
+            pltpu.SemaphoreType.DMA((CHUNKS + 1,)),
+            pltpu.SemaphoreType.DMA((CHUNKS + 1,)),
+            pltpu.SemaphoreType.DMA((CHUNKS,)),
             pltpu.SemaphoreType.DMA((CHUNKS, n_own)),
         ],
         compiler_params=pltpu.CompilerParams(

time: 46.6 us -> 40.2 us (0.86)
  Pallas kernels: 45.1 us -> 38.7 us
    pallas_call x1, Pallas kernels: 45.1 us -> 38.7 us  [layer(): pl.pallas_call(functools.partial(fused, n_kv, n_tp), out_shape=jax.ShapeD...]
where the time goes in v2:
time: 40.2 us; the launch traced here: 40 us
  Pallas kernels  38.7 us (96%)
  local copies, waits for them, and re-layouts  1.28 us (3%)
    pallas_call x1, Pallas kernels, layer(): pl.pallas_call(functools.partial(fused, n_kv, n_tp), out_shape=jax.ShapeD...  38.7 us
    unnamed x1, local copies, waits for them, and re-layouts  1.28 us

profile of v2, /device:TPU:0, one launch (start us, length us, event | category | flops | bytes accessed | tf_op | source)
XLA Modules:
  0.0 40.0 jit_solution(15497301471566647071)
XLA Ops:
  0.0 38.7 %shard_map.145 = bf16[16,128]{1,0:T(8,128)(2,1)} custom-call(bf16[16,128]{1,0:T(8,128)(2,1)} %tokens.1, bf16[4096]{0:T(1024)(128)(2,1)} %gain_attn_any.1, f32[1,32]{1,0:T(1,128)} %bitcast.3, s32[16]{0:T(128)} %lengths_any.1, bf16[4096]{0:T(1024)(128)(2,1)} %gain_mixer_any.1, bf16[512,512]{1,0:T(8,128)(2,1)} %w_query.1, bf16[512,512]{1,0:T(8,128)(2,1)} %w_key.1, ...), custom_call_target="tpu_custom_call" | custom-call | tf_op jit(solution)/shard_map/pallas_call | solution.py:712
  38.7 1.3 %copy.17 = bf16[16,128]{1,0:T(8,128)(2,1)} copy(bf16[16,128]{1,0:T(8,128)(2,1)} %shard_map.145) | data formatting | bytes 8192
